TPU v7x, 32 devices: a whole 2x2x4 slice. The times are simulated.
32 devices in a mesh: ep: 4 (over z), tp: 8 (over y, x, core).
Axes of the slice: x: 2, y: 2, z: 4, core: 2. Of those that a mesh axis runs over, the one named last changes fastest.
Arguments:
- tokens: bfloat16 [640, 2048], P('ep', 'tp'), may hold values from -6 to 6
- cotangent: bfloat16 [640, 2048], P('ep', 'tp'), may hold values from -6 to 6
- routes: int32 [640, 2], P('ep'), may hold values from 0 to 23, all different within a row; in each aligned block of 160 rows (0 to 159, 160 to 319, ...) at most 14 rows name the same one
- gate_weights: float32 [640, 2], P('ep'), may hold values from 0.2 to 2.5
- expert_gate: bfloat16 [24, 2048, 512], P('ep', 'tp'), may hold values from -0.125 to 0.125
- expert_up: bfloat16 [24, 2048, 512], P('ep', 'tp'), may hold values from -0.125 to 0.125
- expert_down: bfloat16 [24, 512, 2048], P('ep', None, 'tp'), may hold values from -0.25 to 0.25
- shared_gate: bfloat16 [2048, 576], P('tp'), may hold values from -0.125 to 0.125
- shared_up: bfloat16 [2048, 576], P('tp'), may hold values from -0.125 to 0.125
- shared_down: bfloat16 [576, 2048], P(None, 'tp'), may hold values from -0.25 to 0.25
Outputs:
- token_grad: bfloat16 [640, 2048], P('ep', 'tp')
- weight_grad: float32 [640, 2], P('ep')
- expert_gate_grad: float32 [24, 2048, 512], P('ep', 'tp')
- expert_up_grad: float32 [24, 2048, 512], P('ep', 'tp')
- expert_down_grad: float32 [24, 512, 2048], P('ep', None, 'tp')
- shared_gate_grad: float32 [2048, 576], P('tp', 'ep')
- shared_up_grad: float32 [2048, 576], P('tp', 'ep')
- shared_down_grad: float32 [576, 2048], P('ep', 'tp')
- gate_rows_sq: float32 [24, 2048], P('ep', 'tp')
- up_rows_sq: float32 [24, 2048], P('ep', 'tp')
- down_rows_sq: float32 [24, 512], P('ep')
- shared_gate_rows_sq: float32 [2048], P('tp')
- shared_up_rows_sq: float32 [2048], P('tp')
- shared_down_rows_sq: float32 [576], P('ep')
Inputs may be any that keep to these rules, and one draw needn't show every extreme that they name: `routes`: each row names 2 different experts. Among the rows of one index of ep (aligned blocks of 160 rows) no expert is named more than 14 times, a bound that some block reaches.
All inputs are finite; a program needn't handle non-finite values.
Results may differ from a plain program's by a relative error of at most 0.0059.
Values may be sent and summed in bfloat16 or wider, within the bound.
A program may use at most 64 MiB of HBM per device.

v0:
```python
import jax
import jax.numpy as jnp
from jax import lax
from jax.sharding import PartitionSpec as P


def silu_parts(pre):
    logistic = jax.nn.sigmoid(pre)
    return (pre * logistic, logistic * (1.0 + pre * (1.0 - logistic)))


def activate(gate_sum, up_sum, back_sum, recv_w, s_gate, s_up, s_back):
    silu_out, silu_slope = silu_parts(gate_sum)
    hidden = (silu_out * up_sum).astype(jnp.bfloat16)
    dhidden = recv_w[:, :, None] * back_sum
    grad_gate = (dhidden * up_sum * silu_slope).astype(jnp.bfloat16)
    grad_up = (dhidden * silu_out).astype(jnp.bfloat16)
    dots = jnp.sum(hidden.astype(jnp.float32) * back_sum, axis=2)
    s_out, s_slope = silu_parts(s_gate)
    s_hidden = (s_out * s_up).astype(jnp.bfloat16)
    s_dgate = (s_back * s_up * s_slope).astype(jnp.bfloat16)
    s_dup = (s_back * s_out).astype(jnp.bfloat16)
    return (hidden, grad_gate, grad_up, dots, s_hidden, s_dgate, s_dup)


def per_device(
    tokens,
    cotangent,
    routes,
    gate_weights,
    expert_gate,
    expert_up,
    expert_down,
    shared_gate,
    shared_up,
    shared_down,
):
    tok_rows, narrow = tokens.shape
    picks_per = routes.shape[1]
    local_experts = expert_gate.shape[0]
    experts_all = local_experts * lax.axis_size("ep")
    capacity = max(2, (tok_rows * picks_per + experts_all - 1) // experts_all)
    owners = routes.reshape(-1)
    assigned = owners.shape[0]
    picked = (owners[:, None] == jnp.arange(experts_all, dtype=jnp.int32)[None, :]).astype(
        jnp.int32
    )
    slot_rank = jnp.sum((jnp.cumsum(picked, axis=0) - picked) * picked, axis=1)
    source_tok = jnp.arange(assigned, dtype=jnp.int32) // picks_per
    slot_tok = (
        jnp.full((capacity, experts_all), tok_rows, jnp.int32).at[slot_rank, owners].set(source_tok)
    )
    slot_weight = (
        jnp.zeros((capacity, experts_all), jnp.float32)
        .at[slot_rank, owners]
        .set(gate_weights.reshape(-1))
    )
    zero_row = jnp.zeros((1, narrow), tokens.dtype)
    sent_x = jnp.concatenate([tokens, zero_row], axis=0)[slot_tok]
    sent_dy = jnp.concatenate([cotangent, zero_row], axis=0)[slot_tok]
    recv_x, recv_dy = (
        lax.all_to_all(sent_x, "ep", split_axis=1, concat_axis=0, tiled=True),
        lax.all_to_all(sent_dy, "ep", split_axis=1, concat_axis=0, tiled=True),
    )
    recv_w = lax.all_to_all(slot_weight, "ep", split_axis=1, concat_axis=0, tiled=True)
    gate_part = jnp.einsum("rel,elf->ref", recv_x, expert_gate, preferred_element_type=jnp.float32)
    up_part = jnp.einsum("rel,elf->ref", recv_x, expert_up, preferred_element_type=jnp.float32)
    back_part = jnp.einsum("rel,efl->ref", recv_dy, expert_down, preferred_element_type=jnp.float32)
    s_gate_part = jnp.dot(tokens, shared_gate, preferred_element_type=jnp.float32)
    s_up_part = jnp.dot(tokens, shared_up, preferred_element_type=jnp.float32)
    s_back_part = jnp.einsum(
        "tl,sl->ts", cotangent, shared_down, preferred_element_type=jnp.float32
    )
    gate_sum, up_sum, back_sum, s_gate, s_up, s_back = lax.psum(
        (gate_part, up_part, back_part, s_gate_part, s_up_part, s_back_part), "tp"
    )
    hidden, grad_gate, grad_up, gate_grad, s_hidden, s_dgate, s_dup = activate(
        gate_sum, up_sum, back_sum, recv_w, s_gate, s_up, s_back
    )
    weighted = (recv_w[:, :, None] * recv_dy.astype(jnp.float32)).astype(jnp.bfloat16)
    down_grad = jnp.einsum("ref,rel->efl", hidden, weighted, preferred_element_type=jnp.float32)
    gate_wgrad = jnp.einsum("rel,ref->elf", recv_x, grad_gate, preferred_element_type=jnp.float32)
    up_wgrad = jnp.einsum("rel,ref->elf", recv_x, grad_up, preferred_element_type=jnp.float32)
    row_grad = (
        jnp.einsum("ref,elf->rel", grad_gate, expert_gate, preferred_element_type=jnp.float32)
        + jnp.einsum("ref,elf->rel", grad_up, expert_up, preferred_element_type=jnp.float32)
    ).astype(jnp.bfloat16)
    back_rows = lax.all_to_all(row_grad, "ep", split_axis=0, concat_axis=1, tiled=True)
    back_gate = lax.all_to_all(gate_grad, "ep", split_axis=0, concat_axis=1, tiled=True)
    flat_index = slot_rank * experts_all + owners
    routed = back_rows.reshape(capacity * experts_all, narrow)[flat_index].astype(jnp.float32)
    routed = routed.reshape(tok_rows, picks_per, narrow).sum(axis=1)
    weight_grad = back_gate.reshape(-1)[flat_index].reshape(tok_rows, picks_per)
    term_gate = jnp.einsum("tl,ts->ls", tokens, s_dgate, preferred_element_type=jnp.float32)
    term_up = jnp.einsum("tl,ts->ls", tokens, s_dup, preferred_element_type=jnp.float32)
    term_down = jnp.einsum("ts,tl->sl", s_hidden, cotangent, preferred_element_type=jnp.float32)
    shared_gate_grad, shared_up_grad, shared_down_grad = (
        lax.psum_scatter(term_gate, "ep", scatter_dimension=1, tiled=True),
        lax.psum_scatter(term_up, "ep", scatter_dimension=1, tiled=True),
        lax.psum_scatter(term_down, "ep", scatter_dimension=0, tiled=True),
    )
    shared_rows = jnp.einsum(
        "ts,ls->tl", s_dgate, shared_gate, preferred_element_type=jnp.float32
    ) + jnp.einsum("ts,ls->tl", s_dup, shared_up, preferred_element_type=jnp.float32)
    token_grad = (routed + shared_rows).astype(jnp.bfloat16)
    gate_rows_sq = jnp.sum(gate_wgrad * gate_wgrad, axis=2)
    up_rows_sq = jnp.sum(up_wgrad * up_wgrad, axis=2)
    down_rows_sq, shared_down_rows_sq = lax.psum(
        (
            jnp.sum(down_grad * down_grad, axis=2),
            jnp.sum(shared_down_grad * shared_down_grad, axis=1),
        ),
        "tp",
    )
    shared_gate_rows_sq, shared_up_rows_sq = lax.psum(
        (
            jnp.sum(shared_gate_grad * shared_gate_grad, axis=1),
            jnp.sum(shared_up_grad * shared_up_grad, axis=1),
        ),
        "ep",
    )
    return (
        token_grad,
        weight_grad,
        gate_wgrad,
        up_wgrad,
        down_grad,
        shared_gate_grad,
        shared_up_grad,
        shared_down_grad,
        gate_rows_sq,
        up_rows_sq,
        down_rows_sq,
        shared_gate_rows_sq,
        shared_up_rows_sq,
        shared_down_rows_sq,
    )


def solution(mesh):
    return jax.shard_map(
        per_device,
        mesh=mesh,
        in_specs=(
            P("ep", "tp"),
            P("ep", "tp"),
            P("ep", None),
            P("ep", None),
            P("ep", "tp", None),
            P("ep", "tp", None),
            P("ep", None, "tp"),
            P("tp", None),
            P("tp", None),
            P(None, "tp"),
        ),
        out_specs=(
            P("ep", "tp"),
            P("ep", None),
            P("ep", "tp", None),
            P("ep", "tp", None),
            P("ep", None, "tp"),
            P("tp", "ep"),
            P("tp", "ep"),
            P("ep", "tp"),
            P("ep", "tp"),
            P("ep", "tp"),
            P("ep", None),
            P("tp"),
            P("tp"),
            P("ep"),
        ),
        check_vma=False,
    )
```

profile of v0, /device:TPU:0, one launch (start us, length us, event | category | flops | bytes accessed | tf_op | source)
XLA Modules:
  0.0 251.2 jit_solution(17227434565805106463)
XLA Ops:
  7.2 0.9 copy.56
  8.1 0.1 eq.22
  8.2 0.1 reshape.138
  8.4 0.9 reduce-window.6
  9.3 0.2 slice_reduce_fusion
  9.7 17.0 %scatter_fusion.1 = s32[14,24]{1,0:T(8,128)S(1)} fusion(s32[14,24]{1,0:T(8,128)S(1)} %broadcast_in_dim.7, s32[320]{0:T(512)S(1)} %get-tuple-element.71, s32[320]{0:T(512)S(1)} %add_select_fusion), kind=kCustom, calls=%fused_computation.5 | custom fusion | bytes 6400 | tf_op jit(solution)/shard_map/scatter | solution.py:51
  26.9 2.0 gather_fusion.1
  29.0 0.7 copy.65
  29.7 6.4 %all-to-all-start.2 = ((bf16[14,24,256]{2,0,1:T(8,128)(2,1)}), bf16[14,24,256]{2,0,1:T(8,128)(2,1)S(1)}, u32[]{:S(2)}, u32[]{:S(2)}) async-start(bf16[14,24,256]{2,0,1:T(8,128)(2,1)} %copy.65), calls=%async_computation.2 | async-start | bytes 393216 | tf_op jit(solution)/shard_map/all_to_all | solution.py:62
  36.0 1.0 fusion.21
  37.0 1.0 fusion.20
  38.1 2.0 gather_fusion
  40.1 0.7 copy.63
  40.8 1.0 fusion.22
  41.9 1.7 all-to-all-done.2
  43.5 4.0 %all-to-all-start.1 = ((bf16[14,24,256]{2,0,1:T(8,128)(2,1)}), bf16[14,24,256]{2,0,1:T(8,128)(2,1)}, u32[]{:S(2)}, u32[]{:S(2)}) async-start(bf16[14,24,256]{2,0,1:T(8,128)(2,1)} %copy.63), calls=%async_computation.1 | async-start | bytes 393216 | tf_op jit(solution)/shard_map/all_to_all | solution.py:63
  47.6 1.7 copy.66
  49.3 1.0 all_to_all.71
  50.3 1.2 convolution_bitcast_fusion
  51.6 1.2 convolution_bitcast_fusion.1
  52.8 1.1 all-to-all-done.1
  53.8 1.6 copy.64
  55.5 1.7 all_to_all.67
  57.1 3.0 %convolution_bitcast_fusion.2 = f32[56,6,512]{2,0,1:T(8,128)} fusion(bf16[56,6,256]{2,0,1:T(8,128)(2,1)} %all_to_all.67, bf16[6,512,256]{2,1,0:T(8,128)(2,1)} %param.16), kind=kOutput, calls=%fused_computation.11 | convolution fusion | flops 88080384 | bytes 2433024 | tf_op jit(solution)/shard_map/rel,efl->ref/dot_general | solution.py:68
  60.2 72.4 %all-reduce.8.cloned.1.call-done = (f32[56,6,512]{2,0,1:T(8,128)}, f32[56,6,512]{2,0,1:T(8,128)}, f32[56,6,512]{2,0,1:T(8,128)}, f32[160,576]{1,0:T(8,128)}, f32[160,576]{1,0:T(8,128)}, /*index=5*/f32[160,576]{1,0:T(8,128)}) async-done(((f32[56,6,512]{2,0,1:T(8,128)}, f32[56,6,512]{2,0,1:T(8,128)}, f32[56,6,512]{2,0,1:T(8,128)}, f32[160,576]{1,0:T(8,128)}, f32[160,576]{1,0:T(8,128)}, ...) | async-done | bytes 3170320 | tf_op jit(solution)/shard_map/psum | solution.py:74
  132.6 2.2 fusion.6
  134.9 0.1 copy.60
  135.0 0.1 reshape.179
  135.2 17.0 %scatter_fusion = f32[14,24]{1,0:T(8,128)S(1)} fusion(f32[14,24]{1,0:T(8,128)S(1)} %broadcast_in_dim.6, s32[320]{0:T(512)S(1)} %get-tuple-element.71, f32[320]{0:T(512)S(1)} %reshape.179), kind=kCustom, calls=%fused_computation.4 | custom fusion | bytes 6400 | tf_op jit(solution)/shard_map/scatter | solution.py:56
  152.2 0.1 copy.61
  152.2 0.6 all_to_all.61
  152.9 4.6 %all-to-all-start = ((f32[14,4,6]{0,2,1:T(8,128)}), f32[14,4,6]{0,2,1:T(8,128)S(1)}, u32[]{:S(2)}, u32[]{:S(2)}) async-start(f32[14,4,6]{0,2,1:T(8,128)} %all_to_all.61), calls=%async_computation | async-start | bytes 32768 | tf_op jit(solution)/shard_map/all_to_all | solution.py:65
  157.5 5.6 %all-to-all-done = f32[14,4,6]{0,2,1:T(8,128)S(1)} async-done(((f32[14,4,6]{0,2,1:T(8,128)}), f32[14,4,6]{0,2,1:T(8,128)S(1)}, u32[]{:S(2)}, u32[]{:S(2)}) %all-to-all-start) | async-done | bytes 1376 | tf_op jit(solution)/shard_map/all_to_all | solution.py:65
  163.1 0.1 mul.95
  163.2 2.1 multiply_convert_fusion.4
  165.3 0.7 copy-done.4
  166.0 1.1 convolution_bitcast_fusion.3
  167.1 2.9 %multiply_reduce_fusion.3 = (f32[56,6]{0,1:T(8,128)S(1)}, bf16[56,6,512]{2,0,1:T(8,128)(2,1)}, bf16[56,6,512]{2,0,1:T(8,128)(2,1)}, bf16[56,6,512]{2,0,1:T(8,128)(2,1)}) fusion(f32[56,6,512]{2,0,1:T(8,128)} %get-tuple-element.76, f32[56,6,512]{2,0,1:T(8,128)} %get-tuple-element.75, f32[56,6,512]{2,0,1:T(8,128)} %get-tuple-element.74, f32[56,6]{0,1:T(8,128)S(1)} %mul.95), kind=kLoop, calls=%fused_computation.20 | loop fusion | flops 3268272 | bytes 3099264 | tf_op jit(solution)/shard_map/reduce_sum | solution.py:18
  170.1 0.6 copy.70
  170.7 3.3 %all-to-all-start.4 = ((f32[4,14,6]{1,2,0:T(8,128)}), f32[4,14,6]{1,2,0:T(8,128)S(1)}, u32[]{:S(2)}, u32[]{:S(2)}) async-start(f32[4,14,6]{1,2,0:T(8,128)} %copy.70), calls=%async_computation.4 | async-start | bytes 32768 | tf_op jit(solution)/shard_map/all_to_all | solution.py:89
  174.0 2.0 convolution_bitcast_fusion.4
  176.0 2.4 fusion.19
  178.4 2.9 %multiply_reduce_fusion.2 = (f32[6,256]{1,0:T(8,128)}, f32[6,256,512]{2,1,0:T(8,128)}) fusion(bf16[56,6,256]{2,0,1:T(8,128)(2,1)S(1)} %all_to_all.71, bf16[56,6,512]{2,0,1:T(8,128)(2,1)S(1)} %copy-done.2), kind=kOutput, calls=%fused_computation.8 | convolution fusion | flops 89651712 | bytes 3667968 | tf_op jit(solution)/shard_map/rel,ref->elf/dot_general | solution.py:82
  181.3 2.5 %multiply_reduce_fusion = (f32[6,512]{1,0:T(8,128)S(1)}, f32[6,512,256]{1,2,0:T(8,128)}) fusion(bf16[56,6,512]{2,0,1:T(8,128)(2,1)S(1)} %copy-done.8, bf16[56,6,256]{2,0,1:T(8,128)(2,1)S(1)} %copy-done.7, f32[56,6]{0,1:T(8,128)S(1)} %mul.95), kind=kOutput, calls=%fused_computation.6 | convolution fusion | flops 89908224 | bytes 3675456 | tf_op jit(solution)/shard_map/ref,rel->efl/dot_general | solution.py:81
  183.9 1.7 fusion.1
  185.5 0.7 copy.67
  186.3 5.0 %all-to-all-start.3 = ((bf16[56,6,256]{2,1,0:T(8,128)(2,1)}), bf16[56,6,256]{2,1,0:T(8,128)(2,1)S(1)}, u32[]{:S(2)}, u32[]{:S(2)}) async-start(bf16[56,6,256]{2,1,0:T(8,128)(2,1)} %copy.67), calls=%async_computation.3 | async-start | bytes 458752 | tf_op jit(solution)/shard_map/all_to_all | solution.py:88
  191.3 3.9 %multiply_reduce_fusion.1 = (f32[6,256]{1,0:T(8,128)}, f32[6,256,512]{2,1,0:T(8,128)}) fusion(bf16[56,6,256]{2,0,1:T(8,128)(2,1)S(1)} %all_to_all.71, bf16[56,6,512]{2,0,1:T(8,128)(2,1)} %get-tuple-element.85), kind=kOutput, calls=%fused_computation.7 | convolution fusion | flops 89651712 | bytes 3667968 | tf_op jit(solution)/shard_map/rel,ref->elf/dot_general | solution.py:83
  195.2 3.6 %copy.73 = f32[6,512,256]{2,1,0:T(8,128)} copy(f32[6,512,256]{1,2,0:T(8,128)} %get-tuple-element.93) | data formatting | bytes 6291456
  198.8 0.2 fusion.23
  199.0 0.1 copy.71
  199.1 0.1 reshape.141
  199.3 2.4 gather_fusion.3
  201.7 0.1 reshape.142
  201.9 0.7 copy.72
  202.6 2.0 gather_fusion.2
  204.6 0.2 reshape.144
  204.8 0.4 reduce_sum.85
  205.2 0.9 fusion.3
  206.1 1.0 multiply_reduce_fusion.4
  207.1 22.9 %all-reduce.3 = (f32[6,512]{1,0:T(8,128)}, f32[144]{0:T(256)}) all-reduce(f32[6,512]{1,0:T(8,128)S(1)} %get-tuple-element.92, f32[144]{0:T(256)S(1)} %multiply_reduce_fusion.4), channel_id=1, replica_groups=mesh['ep'=4,'tp'=8] {'tp'}, use_global_device_ids=true, to_apply=%region_19.20 | all-reduce | flops 3216 | bytes 25728 | tf_op jit(solution)/shard_map/psum | solution.py:108
  230.1 0.9 multiply_reduce_fusion.5
  231.0 0.9 multiply_reduce_fusion.6
  232.0 12.7 %all-reduce.5 = (f32[256]{0:T(256)}, f32[256]{0:T(256)}) all-reduce(f32[256]{0:T(256)S(1)} %multiply_reduce_fusion.6, f32[256]{0:T(256)S(1)} %multiply_reduce_fusion.5), channel_id=1, replica_groups=mesh['ep'=4,'tp'=8] {'ep'}, use_global_device_ids=true, to_apply=%region_21.22 | all-reduce | flops 512 | bytes 4096 | tf_op jit(solution)/shard_map/psum | solution.py:115
  (65 shorter events, 0.8 us)
Async XLA Ops:
  7.2 43.2 %copy-start = (bf16[6,256,512]{2,1,0:T(8,128)(2,1)S(1)}, bf16[6,256,512]{2,1,0:T(8,128)(2,1)}, u32[]{:S(2)}) copy-start(bf16[6,256,512]{2,1,0:T(8,128)(2,1)} %param.14) | copy-start | bytes 4718596
  9.7 17.1 %copy-start.3 = (bf16[160,256]{1,0:T(8,128)(2,1)S(1)}, bf16[160,256]{1,0:T(8,128)(2,1)}, u32[]{:S(2)}) copy-start(bf16[160,256]{1,0:T(8,128)(2,1)} %param.10) | copy-start | bytes 245764
  26.7 9.3 %copy-start.9 = (bf16[256,576]{0,1:T(8,128)(2,1)S(1)}, bf16[256,576]{0,1:T(8,128)(2,1)}, u32[]{:S(2)}) copy-start(bf16[256,576]{0,1:T(8,128)(2,1)} %param.18) | copy-start | bytes 884740
  26.9 10.1 %copy-start.14 = (bf16[160,256]{1,0:T(8,128)(2,1)S(1)}, bf16[160,256]{1,0:T(8,128)(2,1)}, u32[]{:S(2)}) copy-start(bf16[160,256]{1,0:T(8,128)(2,1)} %param.11) | copy-start | bytes 245764
  26.9 10.1 %copy-start.15 = (bf16[576,256]{1,0:T(8,128)(2,1)S(1)}, bf16[576,256]{1,0:T(8,128)(2,1)}, u32[]{:S(2)}) copy-start(bf16[576,256]{1,0:T(8,128)(2,1)} %param.19) | copy-start | bytes 884740
  29.7 13.9 %all-to-all-start.2 = ((bf16[14,24,256]{2,0,1:T(8,128)(2,1)}), bf16[14,24,256]{2,0,1:T(8,128)(2,1)S(1)}, u32[]{:S(2)}, u32[]{:S(2)}) async-start(bf16[14,24,256]{2,0,1:T(8,128)(2,1)} %copy.65), calls=%async_computation.2 | async-start | bytes 393216 | tf_op jit(solution)/shard_map/all_to_all | solution.py:62
  37.0 3.8 %copy-start.11 = (bf16[256,576]{0,1:T(8,128)(2,1)S(1)}, bf16[256,576]{0,1:T(8,128)(2,1)}, u32[]{:S(2)}) copy-start(bf16[256,576]{0,1:T(8,128)(2,1)} %param.17) | copy-start | bytes 884740
  43.5 4.1 %copy-start.13 = (bf16[14,24,256]{2,0,1:T(8,128)(2,1)}, bf16[14,24,256]{2,0,1:T(8,128)(2,1)S(1)}, u32[]{:S(2)}) copy-start(bf16[14,24,256]{2,0,1:T(8,128)(2,1)S(1)} %all-to-all-done.2) | copy-start | bytes 516100
  43.5 10.3 %all-to-all-start.1 = ((bf16[14,24,256]{2,0,1:T(8,128)(2,1)}), bf16[14,24,256]{2,0,1:T(8,128)(2,1)}, u32[]{:S(2)}, u32[]{:S(2)}) async-start(bf16[14,24,256]{2,0,1:T(8,128)(2,1)} %copy.63), calls=%async_computation.1 | async-start | bytes 393216 | tf_op jit(solution)/shard_map/all_to_all | solution.py:63
  47.5 85.1 %all-reduce.8.cloned.1.call-start = ((), (), s32[]{:S(2)}) async-start(), calls=%async_computation.11 | async-start | bytes 6586368 | tf_op jit(solution)/shard_map/psum | solution.py:74
  47.6 4.0 %copy-start.1 = (bf16[6,256,512]{2,1,0:T(8,128)(2,1)S(1)}, bf16[6,256,512]{2,1,0:T(8,128)(2,1)}, u32[]{:S(2)}) copy-start(bf16[6,256,512]{2,1,0:T(8,128)(2,1)} %param.15) | copy-start | bytes 4718596
  60.1 74.8 %copy-start.16 = (f32[160,2]{0,1:T(2,128)S(1)}, f32[160,2]{0,1:T(2,128)}, u32[]{:S(2)}) copy-start(f32[160,2]{0,1:T(2,128)} %param.13) | copy-start | bytes 3844
  60.1 146.0 %reduce-scatter.8.cloned.1.call-start = ((), (), s32[]{:S(2)}) async-start(), calls=%async_computation.10 | async-start | bytes 737280 | tf_op jit(solution)/shard_map/reduce_scatter | solution.py:100
  152.9 10.2 %all-to-all-start = ((f32[14,4,6]{0,2,1:T(8,128)}), f32[14,4,6]{0,2,1:T(8,128)S(1)}, u32[]{:S(2)}, u32[]{:S(2)}) async-start(f32[14,4,6]{0,2,1:T(8,128)} %all_to_all.61), calls=%async_computation | async-start | bytes 32768 | tf_op jit(solution)/shard_map/all_to_all | solution.py:65
  157.5 72.6 %reduce-scatter.6.cloned.1.call-start = ((), (), s32[]{:S(2)}) async-start(), calls=%async_computation.9 | async-start | bytes 737280 | tf_op jit(solution)/shard_map/reduce_scatter | solution.py:99
  165.3 0.7 copy-start.4
  170.7 15.6 %all-to-all-start.4 = ((f32[4,14,6]{1,2,0:T(8,128)}), f32[4,14,6]{1,2,0:T(8,128)S(1)}, u32[]{:S(2)}, u32[]{:S(2)}) async-start(f32[4,14,6]{1,2,0:T(8,128)} %copy.70), calls=%async_computation.4 | async-start | bytes 32768 | tf_op jit(solution)/shard_map/all_to_all | solution.py:89
  174.0 57.1 %reduce-scatter.4.cloned.1.call-start = ((), (), s32[]{:S(2)}) async-start(), calls=%async_computation.8 | async-start | bytes 737280 | tf_op jit(solution)/shard_map/reduce_scatter | solution.py:98
  176.0 2.4 copy-start.2
  178.4 2.9 %copy-start.7 = (bf16[56,6,256]{2,0,1:T(8,128)(2,1)S(1)}, bf16[56,6,256]{2,0,1:T(8,128)(2,1)}, u32[]{:S(2)}) copy-start(bf16[56,6,256]{2,0,1:T(8,128)(2,1)} %all_to_all.67) | copy-start | bytes 516100
  178.4 2.9 %copy-start.8 = (bf16[56,6,512]{2,0,1:T(8,128)(2,1)S(1)}, bf16[56,6,512]{2,0,1:T(8,128)(2,1)}, u32[]{:S(2)}) copy-start(bf16[56,6,512]{2,0,1:T(8,128)(2,1)} %get-tuple-element.83) | copy-start | bytes 1032196
  186.3 16.2 %all-to-all-start.3 = ((bf16[56,6,256]{2,1,0:T(8,128)(2,1)}), bf16[56,6,256]{2,1,0:T(8,128)(2,1)S(1)}, u32[]{:S(2)}, u32[]{:S(2)}) async-start(bf16[56,6,256]{2,1,0:T(8,128)(2,1)} %copy.67), calls=%async_computation.3 | async-start | bytes 458752 | tf_op jit(solution)/shard_map/all_to_all | solution.py:88
  195.2 3.6 %copy-start.6 = (bf16[160,576]{1,0:T(8,128)(2,1)S(1)}, bf16[160,576]{1,0:T(8,128)(2,1)}, u32[]{:S(2)}) copy-start(bf16[160,576]{1,0:T(8,128)(2,1)} %get-tuple-element.87) | copy-start | bytes 552964
  195.2 3.6 %copy-start.12 = (bf16[256,576]{0,1:T(8,128)(2,1)S(1)}, bf16[256,576]{0,1:T(8,128)(2,1)}, u32[]{:S(2)}) copy-start(bf16[256,576]{0,1:T(8,128)(2,1)} %param.17) | copy-start | bytes 884740
  202.5 2.7 %copy-start.5 = (bf16[160,576]{1,0:T(8,128)(2,1)S(1)}, bf16[160,576]{1,0:T(8,128)(2,1)}, u32[]{:S(2)}) copy-start(bf16[160,576]{1,0:T(8,128)(2,1)} %copy-done.4) | copy-start | bytes 552964
  202.5 2.7 %copy-start.10 = (bf16[256,576]{0,1:T(8,128)(2,1)S(1)}, bf16[256,576]{0,1:T(8,128)(2,1)}, u32[]{:S(2)}) copy-start(bf16[256,576]{0,1:T(8,128)(2,1)} %param.18) | copy-start | bytes 884740
Sparse Core Ops, SparseCore 0:
  60.2 72.3 all-reduce.7
  135.5 22.1 reduce-scatter.7
  167.2 19.7 reduce-scatter.5
  189.7 21.0 reduce-scatter.3
where the time goes:
time: 252 us; the launch traced here: 251 us
  waiting for transfers between devices  80.8 us (32%)
  local copies, waits for them, and re-layouts  59.6 us (24%)
  blocking collectives  35.7 us (14%)
  matrix products  28.3 us (11%)
  starting transfers between devices  23.3 us (9%)
  between operations  14.1 us (6%)
  other arithmetic  9.43 us (4%)
    psum x1, waiting for transfers between devices, per_device(): lax.psum((gate_part, up_part, back_part, s_gate_part, s_up_part, s_back_p...  72.4 us
    psum x1, blocking collectives, per_device(): lax.psum((jnp.sum(down_grad * down_grad, axis=2), jnp.sum(shared_down_gra...  22.9 us
    scatter x2, local copies, waits for them, and re-layouts, per_device(): slot_weight = jnp.zeros((capacity, experts_all), jnp.float32).at[slot_ran...  17.1 us
    scatter x1, local copies, waits for them, and re-layouts, per_device(): jnp.full((capacity, experts_all), tok_rows, jnp.int32).at[slot_rank, owners]  17 us
    psum x1, blocking collectives, per_device(): lax.psum((jnp.sum(shared_gate_grad * shared_gate_grad, axis=1), jnp.sum(s...  12.7 us
    all_to_all x1, starting transfers between devices, per_device(): lax.all_to_all(sent_x, 'ep', split_axis=1, concat_axis=0, tiled=True)  6.35 us
    unnamed x38, local copies, waits for them, and re-layouts  6.04 us
    all_to_all x1, waiting for transfers between devices, per_device(): lax.all_to_all(slot_weight, 'ep', split_axis=1, concat_axis=0, tiled=True)  5.6 us
  transfers between devices with their start and end apart: 9, of which 4 were waited for; matrix products, arithmetic and copies ran while one was open for 25% of the time, Pallas kernels for 0%

commit v1 on v0

--- a/solution.py
+++ b/solution.py
@@ -59,7 +59,10 @@
     sent_x = jnp.concatenate([tokens, zero_row], axis=0)[slot_tok]
     sent_dy = jnp.concatenate([cotangent, zero_row], axis=0)[slot_tok]
     recv_x, recv_dy = (
-        lax.all_to_all(sent_x, "ep", split_axis=1, concat_axis=0, tiled=True),
+        jnp.concatenate(
+            lax.all_to_all(jnp.stack(jnp.split(sent_x, lax.axis_size("ep"), axis=1)), "ep", 0, 0),
+            axis=0,
+        ),
         lax.all_to_all(sent_dy, "ep", split_axis=1, concat_axis=0, tiled=True),
     )
     recv_w = lax.all_to_all(slot_weight, "ep", split_axis=1, concat_axis=0, tiled=True)

time: 252 us -> 253 us (level)
  no operation moved by 1% of the time
where the time goes in v1:
time: 253 us; the launch traced here: 252 us
  waiting for transfers between devices  80.8 us (32%)
  local copies, waits for them, and re-layouts  59.6 us (24%)
  blocking collectives  35.7 us (14%)
  matrix products  28.3 us (11%)
  starting transfers between devices  23.3 us (9%)
  between operations  14.1 us (6%)
  other arithmetic  10.1 us (4%)
    psum x1, waiting for transfers between devices, per_device(): lax.psum((gate_part, up_part, back_part, s_gate_part, s_up_part, s_back_p...  72.4 us
    psum x1, blocking collectives, per_device(): lax.psum((jnp.sum(down_grad * down_grad, axis=2), jnp.sum(shared_down_gra...  22.9 us
    scatter x2, local copies, waits for them, and re-layouts, per_device(): slot_weight = jnp.zeros((capacity, experts_all), jnp.float32).at[slot_ran...  17.1 us
    scatter x1, local copies, waits for them, and re-layouts, per_device(): jnp.full((capacity, experts_all), tok_rows, jnp.int32).at[slot_rank, owners]  17 us
    psum x1, blocking collectives, per_device(): lax.psum((jnp.sum(shared_gate_grad * shared_gate_grad, axis=1), jnp.sum(s...  12.7 us
    unnamed x38, local copies, waits for them, and re-layouts  6.71 us
    all_to_all x1, starting transfers between devices, per_device(): lax.all_to_all(jnp.stack(jnp.split(sent_x, lax.axis_size('ep'), axis=1)),...  6.35 us
    all_to_all x1, waiting for transfers between devices, per_device(): lax.all_to_all(slot_weight, 'ep', split_axis=1, concat_axis=0, tiled=True)  5.6 us
  transfers between devices with their start and end apart: 9, of which 4 were waited for; matrix products, arithmetic and copies ran while one was open for 25% of the time, Pallas kernels for 0%

profile of v1, /device:TPU:0, one launch (start us, length us, event | category | flops | bytes accessed | tf_op | source)
XLA Modules:
  0.0 252.0 jit_solution(8376591710789150018)
XLA Ops:
  7.2 0.9 copy.64
  8.1 0.1 eq.22
  8.2 0.1 reshape.141
  8.4 0.9 reduce-window.6
  9.3 0.2 slice_reduce_fusion
  9.7 17.0 %scatter_fusion.1 = s32[14,24]{1,0:T(8,128)S(1)} fusion(s32[14,24]{1,0:T(8,128)S(1)} %broadcast_in_dim.7, s32[320]{0:T(512)S(1)} %get-tuple-element.71, s32[320]{0:T(512)S(1)} %add_select_fusion), kind=kCustom, calls=%fused_computation.5 | custom fusion | bytes 6400 | tf_op jit(solution)/shard_map/scatter | solution.py:51
  26.9 2.0 gather_fusion.1
  29.1 0.7 pad_maximum_fusion
  29.8 6.4 %all-to-all-start.2 = ((bf16[4,14,6,256]{3,1,2,0:T(8,128)(2,1)}), bf16[4,14,6,256]{3,1,2,0:T(8,128)(2,1)S(1)}, u32[]{:S(2)}, u32[]{:S(2)}) async-start(bf16[4,14,6,256]{3,1,2,0:T(8,128)(2,1)} %pad_maximum_fusion), calls=%async_computation.2 | async-start | bytes 393216 | tf_op jit(solution)/shard_map/all_to_all | solution.py:63
  36.1 1.0 fusion.22
  37.2 1.0 fusion.21
  38.2 2.0 gather_fusion
  40.2 0.7 copy.71
  40.9 1.0 fusion.23
  42.0 1.7 all-to-all-done.2
  43.6 0.7 copy-done.13
  44.3 4.0 %all-to-all-start.1 = ((bf16[14,24,256]{2,0,1:T(8,128)(2,1)}), bf16[14,24,256]{2,0,1:T(8,128)(2,1)}, u32[]{:S(2)}, u32[]{:S(2)}) async-start(bf16[14,24,256]{2,0,1:T(8,128)(2,1)} %copy.71), calls=%async_computation.1 | async-start | bytes 393216 | tf_op jit(solution)/shard_map/all_to_all | solution.py:66
  48.4 1.7 copy.77
  50.1 1.0 reshape.143
  51.1 1.2 convolution_bitcast_fusion
  52.3 1.2 convolution_bitcast_fusion.1
  53.6 1.1 all-to-all-done.1
  54.6 1.6 copy.72
  56.3 1.7 all_to_all.57
  57.9 3.0 %convolution_bitcast_fusion.2 = f32[56,6,512]{2,0,1:T(8,128)} fusion(bf16[56,6,256]{2,0,1:T(8,128)(2,1)} %all_to_all.57, bf16[6,512,256]{2,1,0:T(8,128)(2,1)} %param.16), kind=kOutput, calls=%fused_computation.11 | convolution fusion | flops 88080384 | bytes 2433024 | tf_op jit(solution)/shard_map/rel,efl->ref/dot_general | solution.py:71
  61.0 72.4 %all-reduce.8.cloned.1.call-done = (f32[56,6,512]{2,0,1:T(8,128)}, f32[56,6,512]{2,0,1:T(8,128)}, f32[56,6,512]{2,0,1:T(8,128)}, f32[160,576]{1,0:T(8,128)}, f32[160,576]{1,0:T(8,128)}, /*index=5*/f32[160,576]{1,0:T(8,128)}) async-done(((f32[56,6,512]{2,0,1:T(8,128)}, f32[56,6,512]{2,0,1:T(8,128)}, f32[56,6,512]{2,0,1:T(8,128)}, f32[160,576]{1,0:T(8,128)}, f32[160,576]{1,0:T(8,128)}, ...) | async-done | bytes 3170320 | tf_op jit(solution)/shard_map/psum | solution.py:77
  133.4 2.2 fusion.6
  135.7 0.1 copy.68
  135.8 0.1 reshape.183
  135.9 17.0 %scatter_fusion = f32[14,24]{1,0:T(8,128)S(1)} fusion(f32[14,24]{1,0:T(8,128)S(1)} %broadcast_in_dim.6, s32[320]{0:T(512)S(1)} %get-tuple-element.71, f32[320]{0:T(512)S(1)} %reshape.183), kind=kCustom, calls=%fused_computation.4 | custom fusion | bytes 6400 | tf_op jit(solution)/shard_map/scatter | solution.py:56
  152.9 0.1 copy.69
  153.0 0.6 all_to_all.51
  153.6 4.6 %all-to-all-start = ((f32[14,4,6]{0,2,1:T(8,128)}), f32[14,4,6]{0,2,1:T(8,128)S(1)}, u32[]{:S(2)}, u32[]{:S(2)}) async-start(f32[14,4,6]{0,2,1:T(8,128)} %all_to_all.51), calls=%async_computation | async-start | bytes 32768 | tf_op jit(solution)/shard_map/all_to_all | solution.py:68
  158.3 5.6 %all-to-all-done = f32[14,4,6]{0,2,1:T(8,128)S(1)} async-done(((f32[14,4,6]{0,2,1:T(8,128)}), f32[14,4,6]{0,2,1:T(8,128)S(1)}, u32[]{:S(2)}, u32[]{:S(2)}) %all-to-all-start) | async-done | bytes 1376 | tf_op jit(solution)/shard_map/all_to_all | solution.py:68
  163.9 2.1 multiply_convert_fusion.4
  166.1 0.7 copy-done.4
  166.8 1.1 convolution_bitcast_fusion.3
  167.9 2.9 %multiply_reduce_fusion.3 = (f32[56,6]{0,1:T(8,128)S(1)}, bf16[56,6,512]{2,0,1:T(8,128)(2,1)}, bf16[56,6,512]{2,0,1:T(8,128)(2,1)}, bf16[56,6,512]{2,0,1:T(8,128)(2,1)}) fusion(f32[56,6,512]{2,0,1:T(8,128)} %get-tuple-element.76, f32[56,6,512]{2,0,1:T(8,128)} %get-tuple-element.75, f32[56,6,512]{2,0,1:T(8,128)} %get-tuple-element.74, f32[56,6]{0,1:T(8,128)S(1)} %mul.95), kind=kLoop, calls=%fused_computation.20 | loop fusion | flops 3268272 | bytes 3099264 | tf_op jit(solution)/shard_map/reduce_sum | solution.py:18
  170.9 0.6 copy.81
  171.5 3.3 %all-to-all-start.4 = ((f32[4,14,6]{1,2,0:T(8,128)}), f32[4,14,6]{1,2,0:T(8,128)S(1)}, u32[]{:S(2)}, u32[]{:S(2)}) async-start(f32[4,14,6]{1,2,0:T(8,128)} %copy.81), calls=%async_computation.4 | async-start | bytes 32768 | tf_op jit(solution)/shard_map/all_to_all | solution.py:92
  174.8 2.0 convolution_bitcast_fusion.4
  176.8 2.4 fusion.20
  179.2 2.9 %multiply_reduce_fusion.2 = (f32[6,256]{1,0:T(8,128)}, f32[6,256,512]{2,1,0:T(8,128)}) fusion(bf16[56,6,256]{2,0,1:T(8,128)(2,1)S(1)} %reshape.143, bf16[56,6,512]{2,0,1:T(8,128)(2,1)S(1)} %copy-done.2), kind=kOutput, calls=%fused_computation.8 | convolution fusion | flops 89651712 | bytes 3667968 | tf_op jit(solution)/shard_map/rel,ref->elf/dot_general | solution.py:85
  182.1 2.5 %multiply_reduce_fusion = (f32[6,512]{1,0:T(8,128)S(1)}, f32[6,512,256]{1,2,0:T(8,128)}) fusion(bf16[56,6,512]{2,0,1:T(8,128)(2,1)S(1)} %copy-done.8, bf16[56,6,256]{2,0,1:T(8,128)(2,1)S(1)} %copy-done.7, f32[56,6]{0,1:T(8,128)S(1)} %mul.95), kind=kOutput, calls=%fused_computation.6 | convolution fusion | flops 89908224 | bytes 3675456 | tf_op jit(solution)/shard_map/ref,rel->efl/dot_general | solution.py:84
  184.6 1.7 fusion.1
  186.3 0.7 copy.78
  187.1 5.0 %all-to-all-start.3 = ((bf16[56,6,256]{2,1,0:T(8,128)(2,1)}), bf16[56,6,256]{2,1,0:T(8,128)(2,1)S(1)}, u32[]{:S(2)}, u32[]{:S(2)}) async-start(bf16[56,6,256]{2,1,0:T(8,128)(2,1)} %copy.78), calls=%async_computation.3 | async-start | bytes 458752 | tf_op jit(solution)/shard_map/all_to_all | solution.py:91
  192.1 3.9 %multiply_reduce_fusion.1 = (f32[6,256]{1,0:T(8,128)}, f32[6,256,512]{2,1,0:T(8,128)}) fusion(bf16[56,6,256]{2,0,1:T(8,128)(2,1)S(1)} %reshape.143, bf16[56,6,512]{2,0,1:T(8,128)(2,1)} %get-tuple-element.85), kind=kOutput, calls=%fused_computation.7 | convolution fusion | flops 89651712 | bytes 3667968 | tf_op jit(solution)/shard_map/rel,ref->elf/dot_general | solution.py:86
  195.9 3.6 %copy.84 = f32[6,512,256]{2,1,0:T(8,128)} copy(f32[6,512,256]{1,2,0:T(8,128)} %get-tuple-element.97) | data formatting | bytes 6291456
  199.6 0.2 fusion.24
  199.8 0.1 copy.82
  199.9 0.1 reshape.145
  200.0 2.4 gather_fusion.3
  202.5 0.1 reshape.146
  202.6 0.7 copy.83
  203.4 2.0 gather_fusion.2
  205.4 0.2 reshape.148
  205.6 0.4 reduce_sum.85
  206.0 0.9 fusion.3
  206.9 1.0 multiply_reduce_fusion.4
  207.9 22.9 %all-reduce.3 = (f32[6,512]{1,0:T(8,128)}, f32[144]{0:T(256)}) all-reduce(f32[6,512]{1,0:T(8,128)S(1)} %get-tuple-element.96, f32[144]{0:T(256)S(1)} %multiply_reduce_fusion.4), channel_id=1, replica_groups=mesh['ep'=4,'tp'=8] {'tp'}, use_global_device_ids=true, to_apply=%region_19.20 | all-reduce | flops 3216 | bytes 25728 | tf_op jit(solution)/shard_map/psum | solution.py:111
  230.8 0.9 multiply_reduce_fusion.5
  231.8 0.9 multiply_reduce_fusion.6
  232.8 12.7 %all-reduce.5 = (f32[256]{0:T(256)}, f32[256]{0:T(256)}) all-reduce(f32[256]{0:T(256)S(1)} %multiply_reduce_fusion.6, f32[256]{0:T(256)S(1)} %multiply_reduce_fusion.5), channel_id=1, replica_groups=mesh['ep'=4,'tp'=8] {'ep'}, use_global_device_ids=true, to_apply=%region_21.22 | all-reduce | flops 512 | bytes 4096 | tf_op jit(solution)/shard_map/psum | solution.py:118
  (68 shorter events, 0.9 us)
Async XLA Ops:
  7.2 43.9 %copy-start = (bf16[6,256,512]{2,1,0:T(8,128)(2,1)S(1)}, bf16[6,256,512]{2,1,0:T(8,128)(2,1)}, u32[]{:S(2)}) copy-start(bf16[6,256,512]{2,1,0:T(8,128)(2,1)} %param.14) | copy-start | bytes 4718596
  9.7 17.1 %copy-start.3 = (bf16[160,256]{1,0:T(8,128)(2,1)S(1)}, bf16[160,256]{1,0:T(8,128)(2,1)}, u32[]{:S(2)}) copy-start(bf16[160,256]{1,0:T(8,128)(2,1)} %param.10) | copy-start | bytes 245764
  26.9 9.2 %copy-start.9 = (bf16[256,576]{0,1:T(8,128)(2,1)S(1)}, bf16[256,576]{0,1:T(8,128)(2,1)}, u32[]{:S(2)}) copy-start(bf16[256,576]{0,1:T(8,128)(2,1)} %param.18) | copy-start | bytes 884740
  28.9 8.2 %copy-start.14 = (bf16[160,256]{1,0:T(8,128)(2,1)S(1)}, bf16[160,256]{1,0:T(8,128)(2,1)}, u32[]{:S(2)}) copy-start(bf16[160,256]{1,0:T(8,128)(2,1)} %param.11) | copy-start | bytes 245764
  28.9 8.2 %copy-start.15 = (bf16[576,256]{1,0:T(8,128)(2,1)S(1)}, bf16[576,256]{1,0:T(8,128)(2,1)}, u32[]{:S(2)}) copy-start(bf16[576,256]{1,0:T(8,128)(2,1)} %param.19) | copy-start | bytes 884740
  29.8 13.9 %all-to-all-start.2 = ((bf16[4,14,6,256]{3,1,2,0:T(8,128)(2,1)}), bf16[4,14,6,256]{3,1,2,0:T(8,128)(2,1)S(1)}, u32[]{:S(2)}, u32[]{:S(2)}) async-start(bf16[4,14,6,256]{3,1,2,0:T(8,128)(2,1)} %pad_maximum_fusion), calls=%async_computation.2 | async-start | bytes 393216 | tf_op jit(solution)/shard_map/all_to_all | solution.py:63
  37.2 3.8 %copy-start.11 = (bf16[256,576]{0,1:T(8,128)(2,1)S(1)}, bf16[256,576]{0,1:T(8,128)(2,1)}, u32[]{:S(2)}) copy-start(bf16[256,576]{0,1:T(8,128)(2,1)} %param.17) | copy-start | bytes 884740
  43.6 0.7 copy-start.13
  44.3 10.3 %all-to-all-start.1 = ((bf16[14,24,256]{2,0,1:T(8,128)(2,1)}), bf16[14,24,256]{2,0,1:T(8,128)(2,1)}, u32[]{:S(2)}, u32[]{:S(2)}) async-start(bf16[14,24,256]{2,0,1:T(8,128)(2,1)} %copy.71), calls=%async_computation.1 | async-start | bytes 393216 | tf_op jit(solution)/shard_map/all_to_all | solution.py:66
  48.3 4.0 %copy-start.1 = (bf16[6,256,512]{2,1,0:T(8,128)(2,1)S(1)}, bf16[6,256,512]{2,1,0:T(8,128)(2,1)}, u32[]{:S(2)}) copy-start(bf16[6,256,512]{2,1,0:T(8,128)(2,1)} %param.15) | copy-start | bytes 4718596
  48.3 85.1 %all-reduce.8.cloned.1.call-start = ((), (), s32[]{:S(2)}) async-start(), calls=%async_computation.11 | async-start | bytes 6586368 | tf_op jit(solution)/shard_map/psum | solution.py:77
  60.9 74.8 %copy-start.16 = (f32[160,2]{0,1:T(2,128)S(1)}, f32[160,2]{0,1:T(2,128)}, u32[]{:S(2)}) copy-start(f32[160,2]{0,1:T(2,128)} %param.13) | copy-start | bytes 3844
  60.9 146.0 %reduce-scatter.8.cloned.1.call-start = ((), (), s32[]{:S(2)}) async-start(), calls=%async_computation.10 | async-start | bytes 737280 | tf_op jit(solution)/shard_map/reduce_scatter | solution.py:103
  153.6 10.2 %all-to-all-start = ((f32[14,4,6]{0,2,1:T(8,128)}), f32[14,4,6]{0,2,1:T(8,128)S(1)}, u32[]{:S(2)}, u32[]{:S(2)}) async-start(f32[14,4,6]{0,2,1:T(8,128)} %all_to_all.51), calls=%async_computation | async-start | bytes 32768 | tf_op jit(solution)/shard_map/all_to_all | solution.py:68
  158.2 72.6 %reduce-scatter.6.cloned.1.call-start = ((), (), s32[]{:S(2)}) async-start(), calls=%async_computation.9 | async-start | bytes 737280 | tf_op jit(solution)/shard_map/reduce_scatter | solution.py:102
  166.1 0.7 copy-start.4
  171.5 15.6 %all-to-all-start.4 = ((f32[4,14,6]{1,2,0:T(8,128)}), f32[4,14,6]{1,2,0:T(8,128)S(1)}, u32[]{:S(2)}, u32[]{:S(2)}) async-start(f32[4,14,6]{1,2,0:T(8,128)} %copy.81), calls=%async_computation.4 | async-start | bytes 32768 | tf_op jit(solution)/shard_map/all_to_all | solution.py:92
  174.7 57.1 %reduce-scatter.4.cloned.1.call-start = ((), (), s32[]{:S(2)}) async-start(), calls=%async_computation.8 | async-start | bytes 737280 | tf_op jit(solution)/shard_map/reduce_scatter | solution.py:101
  176.8 2.4 copy-start.2
  179.2 2.9 %copy-start.7 = (bf16[56,6,256]{2,0,1:T(8,128)(2,1)S(1)}, bf16[56,6,256]{2,0,1:T(8,128)(2,1)}, u32[]{:S(2)}) copy-start(bf16[56,6,256]{2,0,1:T(8,128)(2,1)} %all_to_all.57) | copy-start | bytes 516100
  179.2 2.9 %copy-start.8 = (bf16[56,6,512]{2,0,1:T(8,128)(2,1)S(1)}, bf16[56,6,512]{2,0,1:T(8,128)(2,1)}, u32[]{:S(2)}) copy-start(bf16[56,6,512]{2,0,1:T(8,128)(2,1)} %get-tuple-element.83) | copy-start | bytes 1032196
  187.1 16.2 %all-to-all-start.3 = ((bf16[56,6,256]{2,1,0:T(8,128)(2,1)}), bf16[56,6,256]{2,1,0:T(8,128)(2,1)S(1)}, u32[]{:S(2)}, u32[]{:S(2)}) async-start(bf16[56,6,256]{2,1,0:T(8,128)(2,1)} %copy.78), calls=%async_computation.3 | async-start | bytes 458752 | tf_op jit(solution)/shard_map/all_to_all | solution.py:91
  195.9 3.6 %copy-start.6 = (bf16[160,576]{1,0:T(8,128)(2,1)S(1)}, bf16[160,576]{1,0:T(8,128)(2,1)}, u32[]{:S(2)}) copy-start(bf16[160,576]{1,0:T(8,128)(2,1)} %get-tuple-element.87) | copy-start | bytes 552964
  195.9 3.6 %copy-start.12 = (bf16[256,576]{0,1:T(8,128)(2,1)S(1)}, bf16[256,576]{0,1:T(8,128)(2,1)}, u32[]{:S(2)}) copy-start(bf16[256,576]{0,1:T(8,128)(2,1)} %param.17) | copy-start | bytes 884740
  203.3 2.7 %copy-start.5 = (bf16[160,576]{1,0:T(8,128)(2,1)S(1)}, bf16[160,576]{1,0:T(8,128)(2,1)}, u32[]{:S(2)}) copy-start(bf16[160,576]{1,0:T(8,128)(2,1)} %copy-done.4) | copy-start | bytes 552964
  203.3 2.7 %copy-start.10 = (bf16[256,576]{0,1:T(8,128)(2,1)S(1)}, bf16[256,576]{0,1:T(8,128)(2,1)}, u32[]{:S(2)}) copy-start(bf16[256,576]{0,1:T(8,128)(2,1)} %param.18) | copy-start | bytes 884740
Sparse Core Ops, SparseCore 0:
  61.0 72.3 all-reduce.7
  136.2 22.1 reduce-scatter.7
  168.0 19.6 reduce-scatter.5
  190.5 21.0 reduce-scatter.3
